TPU v7x, 32 devices: a whole 2x2x4 slice. The times are simulated.
32 devices in a mesh: fs: 8 (over z, y), tp: 4 (over x, core).
Axes of the slice: x: 2, y: 2, z: 4, core: 2. Of those that a mesh axis runs over, the one named last changes fastest.
Arguments:
- prompt_tokens: bfloat16 [768, 4096], P('tp'), may hold values from -6 to 6
- norm_gain: float32 [4096], P('fs'), may hold values from 0.1 to 1.9
- gate_trained: float32 [4096, 11264], P('fs', 'tp'), may hold values from -0.09375 to 0.09375
- up_trained: float32 [4096, 11264], P('fs', 'tp'), may hold values from -0.09375 to 0.09375
- down_trained: float32 [11264, 4096], P('fs', 'tp'), may hold values from -0.078125 to 0.078125
Outputs:
- gate_serving: bfloat16 [4096, 11264], P(None, 'fs')
- up_serving: bfloat16 [4096, 11264], P(None, 'fs')
- down_serving: bfloat16 [11264, 4096], P('fs')
- mixed: bfloat16 [768, 4096], P('tp', 'fs')
All inputs are finite; a program needn't handle non-finite values.
Results may differ from a plain program's by a relative error of at most 0.0082.
Values may be sent and summed in bfloat16 or wider, within the bound.
A program may use at most 128 MiB of HBM per device.

v0:
```python
import functools

import jax
import jax.numpy as jnp
from jax import lax
from jax.experimental import pallas as pl
from jax.experimental.pallas import tpu as pltpu
from jax.sharding import PartitionSpec as P

MESH = pl.DeviceIdType.MESH
HOME, AWAY, BOTH = 0, 1, 2


SHARES = ((1, AWAY), (2, BOTH), (4, AWAY), (7, HOME), (6, BOTH), (6, BOTH), (6, BOTH))


def chunk_plan(rows):
    unit = max(16, rows // sum(share for share, _ in SHARES) // 16 * 16)
    plan, at = [], 0
    for i, (share, way) in enumerate(SHARES):
        size = rows - at if i == len(SHARES) - 1 else share * unit
        plan.append((at, size, way))
        at += size
    return tuple(plan)


def exchange_kernel(fs, tp, plan, wg, wu, d, out, dout, part, wbuf, dbuf,
                    part_send, part_recv, own_send, relay_send, land_recv,
                    sib_send, sib_recv, cross_send, down_send, down_recv, local_sem):
    f, t = lax.axis_index("fs"), lax.axis_index("tp")
    x, c = t // 2, lax.rem(t, 2)
    w = (wg, wu)
    rows, width = wg.shape[0], out.shape[2]
    dcols = d.shape[1]
    sib, far = 2 * x + 1 - c, 2 * (1 - x) + c
    chunks = len(plan)

    me = f * tp + t
    barrier = pltpu.get_barrier_semaphore()
    for i in range(1, fs * tp):
        other = lax.rem(me + i, fs * tp)
        pl.semaphore_signal(barrier, inc=1, device_id=(other // tp, lax.rem(other, tp)), device_id_type=MESH)
    pl.semaphore_wait(barrier, fs * tp - 1)

    half = fs // 2
    own_cross = (f // half) != x
    part_cross = (f // half) == x
    true = f >= 0

    def uses(cross, way, dropped):
        return jnp.logical_not(cross) if way == dropped else true

    def remote(src, dst, ssem, rsem, fs_to, tp_to):
        return pltpu.make_async_remote_copy(
            src_ref=src, dst_ref=dst, send_sem=ssem, recv_sem=rsem,
            device_id=(fs_to, tp_to), device_id_type=MESH)

    sent = []

    def send(cond, copy):
        @pl.when(cond)
        def _():
            copy.start()
        sent.append((cond, copy))

    def to_serve(view, sems, k, cond, home):
        at, size, _ = plan[k]
        for y in range(2):
            to = 2 * home + y
            for g in range(2):
                here = jnp.logical_and(to == f, c == g)
                send(jnp.logical_and(cond, jnp.logical_not(here)), remote(
                    view(g, pl.ds(at, size), pl.ds(y * width, width)),
                    out.at[g, pl.ds(f * rows + at, size), :],
                    sems.at[g, y, k], land_recv.at[f, k], to, 2 * x + g))

    def part_copy(g, k):
        at, size, _ = plan[k]
        return remote(w[g].at[pl.ds(at, size), :], part.at[g, pl.ds(at, size), :],
                      part_send.at[g, k], part_recv.at[g, k], f, far)

    for k in range(chunks):
        for g in range(2):
            send(uses(own_cross, plan[k][2], HOME), part_copy(g, k))
    for k in range(chunks):
        to_serve(lambda g, r, q: w[g].at[r, q], own_send, k, uses(own_cross, plan[k][2], AWAY), t)
    block = pl.ds(pl.multiple_of(t * dcols, dcols), dcols)
    down_far = remote(d, dout.at[:, block], down_send.at[0], down_recv.at[0], f, far)
    down_sib = remote(d, dout.at[:, block], down_send.at[1], down_recv.at[1], f, sib)
    send(true, down_far)
    send(true, down_sib)
    take = pltpu.make_async_copy(d, dbuf, local_sem.at[0])
    take.start()
    take.wait()
    put_down = pltpu.make_async_copy(dbuf, dout.at[:, block], local_sem.at[0])
    put_down.start()

    for k in range(chunks):
        come = uses(part_cross, plan[k][2], HOME)

        @pl.when(come)
        def _():
            for g in range(2):
                part_copy(g, k).wait_recv()
        to_serve(lambda g, r, q: part.at[g, r, q], relay_send, k, come, lax.rem(t + 2, tp))

    keeps = lax.rem(f // 2, 2) == c
    at_home = (f // half) == x
    cols = pl.ds(pl.multiple_of(lax.rem(f, 2) * width, width), width)
    mine = pl.ds(f * rows, rows)
    put = pltpu.make_async_copy(wbuf, out.at[c, mine, :], local_sem.at[1])

    @pl.when(keeps)
    def _():
        for g in range(2):
            @pl.when(jnp.logical_and(at_home, c == g))
            def _():
                get = pltpu.make_async_copy(w[g].at[:, cols], wbuf, local_sem.at[1])
                get.start()
                get.wait()

        @pl.when(jnp.logical_not(at_home))
        def _():
            get = pltpu.make_async_copy(part.at[c, :, cols], wbuf, local_sem.at[1])
            get.start()
            get.wait()
        put.start()
        put.wait()

    def landed(g, k, source):
        at, size, _ = plan[k]
        return out.at[g, pl.ds(source * rows + at, size), :]

    def down_on():
        remote(d, dout.at[:, block], down_send.at[0], down_recv.at[0], f, far).wait_recv()
        fblock = pl.ds(pl.multiple_of(far * dcols, dcols), dcols)
        send(true, remote(dout.at[:, fblock], dout.at[:, fblock], down_send.at[2], down_recv.at[2], f, sib))

    def arrive(k, source, cond, cross):
        ref = landed(c, k, source)
        crossed = remote(ref, ref, cross_send.at[source, k], land_recv.at[source, k], f, far)
        kept = jnp.logical_and(keeps, f == source)

        @pl.when(jnp.logical_and(cond, jnp.logical_not(kept)))
        def _():
            crossed.wait_recv()
        if cross:
            send(cond, crossed)
        send(cond, remote(ref, ref, sib_send.at[source, k], sib_recv.at[source, k], f, sib))

    def turns(source):
        return (source // half) != (f // half)

    def side(k):
        return at_home if plan[k][2] == HOME else jnp.logical_not(at_home)

    one_way = [k for k in range(chunks) if plan[k][2] != BOTH]
    both_ways = [k for k in range(chunks) if plan[k][2] == BOTH]
    for k in one_way:
        for source in range(fs):
            arrive(k, source, jnp.logical_and(turns(source), side(k)), True)
    for k in one_way:
        for source in range(fs):
            arrive(k, source, jnp.logical_not(turns(source)), False)
    for k in both_ways:
        if k == both_ways[-1]:
            down_on()
        for source in range(fs):
            arrive(k, source, true, False)
    for k in one_way:
        for source in range(fs):
            arrive(k, source, jnp.logical_and(turns(source), jnp.logical_not(side(k))), False)

    for k in range(chunks):
        for source in range(fs):
            ref = landed(1 - c, k, source)
            remote(ref, ref, sib_send.at[source, k], sib_recv.at[source, k], f, sib).wait_recv()
    put_down.wait()
    down_sib.wait_recv()
    remote(dout.at[:, block], dout.at[:, block], down_send.at[2], down_recv.at[2], f, sib).wait_recv()
    for cond, copy in sent:
        @pl.when(cond)
        def _():
            copy.wait_send()


def exchange(wg, wu, d, fs, tp):
    rows, wide = wg.shape
    width = wide * tp // fs
    plan = chunk_plan(rows)
    n = len(plan)
    dma = pltpu.SemaphoreType.DMA
    any_space = pl.BlockSpec(memory_space=pl.ANY)
    return pl.pallas_call(
        functools.partial(exchange_kernel, fs, tp, plan),
        out_shape=(
            jax.ShapeDtypeStruct((2, rows * fs, width), wg.dtype),
            jax.ShapeDtypeStruct((d.shape[0], d.shape[1] * tp), d.dtype),
            jax.ShapeDtypeStruct((2, rows, wide), wg.dtype),
        ),
        in_specs=[any_space] * 3,
        out_specs=(any_space,) * 3,
        scratch_shapes=[
            pltpu.VMEM((rows, width), wg.dtype),
            pltpu.VMEM(d.shape, d.dtype),
            dma((2, n)), dma((2, n)), dma((2, 2, n)), dma((2, 2, n)), dma((fs, n)),
            dma((fs, n)), dma((fs, n)), dma((fs, n)), dma((3,)), dma((3,)), dma((2,)),
        ],
        compiler_params=pltpu.CompilerParams(collective_id=0, has_side_effects=True),
    )(wg, wu, d)


def hidden_kernel(tok, both, gate_out, up_out, hidden, acc, scale):
    i = pl.program_id(0)
    depth = gate_out.shape[0]

    @pl.when(i == 0)
    def _():
        t = tok[...].astype(jnp.float32)
        scale[...] = lax.rsqrt(jnp.mean(t * t, axis=-1, keepdims=True) + 1e-06)
        acc[...] = jnp.zeros_like(acc)

    gate_out[...] = both[0]
    up_out[...] = both[1]
    piece = tok[:, pl.ds(pl.multiple_of(i * depth, depth), depth)].astype(jnp.float32)
    normed = (piece * scale[...]).astype(jnp.bfloat16)
    for g in range(2):
        acc[g] += jnp.dot(normed, both[g], preferred_element_type=jnp.float32)

    @pl.when(i == pl.num_programs(0) - 1)
    def _():
        hidden[...] = (jax.nn.silu(acc[0]) * acc[1]).astype(hidden.dtype)


def hidden_units(tok, both, steps):
    _, features, width = both.shape
    depth = features // steps
    serving = jax.ShapeDtypeStruct((features, width), both.dtype)
    return pl.pallas_call(
        hidden_kernel,
        grid=(steps,),
        out_shape=(serving, serving, jax.ShapeDtypeStruct((tok.shape[0], width), both.dtype)),
        in_specs=[
            pl.BlockSpec(tok.shape, lambda i: (0, 0)),
            pl.BlockSpec((2, depth, width), lambda i: (0, i, 0)),
        ],
        out_specs=(
            pl.BlockSpec((depth, width), lambda i: (i, 0)),
            pl.BlockSpec((depth, width), lambda i: (i, 0)),
            pl.BlockSpec((tok.shape[0], width), lambda i: (0, 0)),
        ),
        scratch_shapes=[
            pltpu.VMEM((2, tok.shape[0], width), jnp.float32),
            pltpu.VMEM((tok.shape[0], 1), jnp.float32),
        ],
        compiler_params=pltpu.CompilerParams(dimension_semantics=("arbitrary",)),
    )(tok, both)


def partial_kernel(hidden, down, down_out, partial):
    down_out[...] = down[...]
    partial[0] = jnp.dot(hidden[...], down[...], preferred_element_type=jnp.float32).astype(partial.dtype)


def partial_sums(hidden, down, blocks):
    units, features = down.shape
    width = features // blocks
    return pl.pallas_call(
        partial_kernel,
        grid=(blocks,),
        out_shape=(
            jax.ShapeDtypeStruct(down.shape, down.dtype),
            jax.ShapeDtypeStruct((blocks, hidden.shape[0], width), jnp.bfloat16),
        ),
        in_specs=[
            pl.BlockSpec(hidden.shape, lambda j: (0, 0)),
            pl.BlockSpec((units, width), lambda j: (0, j)),
        ],
        out_specs=(
            pl.BlockSpec((units, width), lambda j: (0, j)),
            pl.BlockSpec((1, hidden.shape[0], width), lambda j: (j, 0, 0)),
        ),
        compiler_params=pltpu.CompilerParams(dimension_semantics=("arbitrary",)),
    )(hidden, down)


def reduce_kernel(fs, p, mixed, ybuf, sbuf, zbuf, ysend, yrecv, zsend, zrecv):
    f, t = lax.axis_index("fs"), lax.axis_index("tp")
    z, y = f // 2, lax.rem(f, 2)
    planes = fs // 2
    barrier = pltpu.get_barrier_semaphore()
    for i in range(1, fs):
        pl.semaphore_signal(barrier, inc=1, device_id=(lax.rem(f + i, fs), t), device_id_type=MESH)
    pl.semaphore_wait(barrier, fs - 1)

    def remote(src, dst, ssem, rsem, to):
        return pltpu.make_async_remote_copy(
            src_ref=src, dst_ref=dst, send_sem=ssem, recv_sem=rsem,
            device_id=(to, t), device_id_type=MESH)

    order = sorted(range(1, planes), key=lambda o: abs(o - planes // 2)) + [0]
    across, along = {}, {}
    for off in order:
        to = lax.rem(z + off, planes)
        across[off] = remote(p.at[2 * to + 1 - y], ybuf.at[off], ysend.at[off], yrecv.at[off], 2 * z + 1 - y)
        across[off].start()
    for off in order:
        to = lax.rem(z + off, planes)
        across[off].wait_recv()
        pair = p[2 * to + y].astype(jnp.float32) + ybuf[off].astype(jnp.float32)
        if off:
            sbuf[off] = pair.astype(sbuf.dtype)
            along[off] = remote(sbuf.at[off], zbuf.at[off], zsend.at[off], zrecv.at[off], 2 * to + y)
            along[off].start()
        else:
            total = pair
    for off in order[:-1]:
        along[off].wait_recv()
        total += zbuf[off].astype(jnp.float32)
    mixed[...] = total.astype(mixed.dtype)
    for off in order:
        across[off].wait_send()
        if off:
            along[off].wait_send()


def reduce_over_fs(p, fs):
    _, tokens, width = p.shape
    dma = pltpu.SemaphoreType.DMA
    slots = pltpu.VMEM((fs // 2, tokens, width), p.dtype)
    return pl.pallas_call(
        functools.partial(reduce_kernel, fs),
        out_shape=jax.ShapeDtypeStruct((tokens, width), jnp.bfloat16),
        in_specs=[pl.BlockSpec(memory_space=pltpu.VMEM)],
        out_specs=pl.BlockSpec(memory_space=pltpu.VMEM),
        scratch_shapes=[slots, slots, slots] + [dma((fs // 2,))] * 4,
        compiler_params=pltpu.CompilerParams(collective_id=1, has_side_effects=True),
    )(p)


def by_kernels(prompt_tokens, gate_cast, up_cast, down_cast):
    fs, tp = lax.axis_size("fs"), lax.axis_size("tp")
    both, down_all, _ = exchange(gate_cast, up_cast, down_cast, fs, tp)
    gate_serving, up_serving, hidden = hidden_units(prompt_tokens, both, fs)
    down_serving, partial = partial_sums(hidden, down_all, fs)
    return gate_serving, up_serving, down_serving, reduce_over_fs(partial, fs)


def gather_by_collectives(gate_cast, up_cast, down_cast):
    fs_count = lax.axis_size("fs")
    down_serving = lax.all_gather(down_cast, "tp", axis=1, tiled=True)

    def serve(cast):
        part = lax.all_to_all(cast, "tp", split_axis=0, concat_axis=1, tiled=True)
        mid = lax.all_to_all(part, "fs", split_axis=1, concat_axis=0, tiled=True)
        share, width = mid.shape[0] // fs_count, mid.shape[1]
        blocks = lax.all_gather(mid.reshape(fs_count, share, width), "tp", axis=1, tiled=True)
        return blocks.reshape(-1, width)

    return serve(gate_cast), serve(up_cast), down_serving


def on_device(prompt_tokens, norm_gain, gate_trained, up_trained, down_trained):
    fs, tp = lax.axis_size("fs"), lax.axis_size("tp")
    gate_cast = (gate_trained * norm_gain[:, None]).astype(jnp.bfloat16)
    up_cast = (up_trained * norm_gain[:, None]).astype(jnp.bfloat16)
    down_cast = down_trained.astype(jnp.bfloat16)
    routed = fs == 2 * tp and tp == 4
    if routed:
        return by_kernels(prompt_tokens, gate_cast, up_cast, down_cast)
    gate_serving, up_serving, down_serving = gather_by_collectives(gate_cast, up_cast, down_cast)
    tokens = prompt_tokens.astype(jnp.float32)
    scale = lax.rsqrt(jnp.mean(tokens * tokens, axis=-1, keepdims=True) + 1e-06)
    normed = (tokens * scale).astype(jnp.bfloat16)
    contract = (((0,), (1,)), ((), ()))
    gate_cols = lax.dot_general(gate_serving, normed, contract, preferred_element_type=jnp.float32)
    up_cols = lax.dot_general(up_serving, normed, contract, preferred_element_type=jnp.float32)
    hidden_cols = (jax.nn.silu(gate_cols) * up_cols).astype(jnp.bfloat16)
    summed = lax.psum_scatter(
        lax.dot_general(
            down_serving, hidden_cols, (((0,), (0,)), ((), ())), preferred_element_type=jnp.float32
        ),
        "fs",
        scatter_dimension=0,
        tiled=True,
    )
    mixed = summed.T.astype(jnp.bfloat16)
    return (gate_serving, up_serving, down_serving, mixed)


def solution(mesh):
    return jax.shard_map(
        on_device,
        mesh=mesh,
        in_specs=(P("tp", None), P("fs"), P("fs", "tp"), P("fs", "tp"), P("fs", "tp")),
        out_specs=(P(None, "fs"), P(None, "fs"), P("fs", None), P("tp", "fs")),
        check_vma=False,
    )
```

profile of v0, /device:TPU:0, one launch (start us, length us, event | category | flops | bytes accessed | tf_op | source)
XLA Modules:
  0.0 301.0 jit_solution(13775465769781417125)
XLA Ops:
  0.6 0.0 copy-start
  0.6 0.0 copy-start.1
  0.7 4.8 %convert_element_type.11.d = bf16[1408,1024]{1,0:T(8,128)(2,1)} convert(f32[1408,1024]{1,0:T(8,128)} %param.9) | non-fusion elementwise | flops 1441792 | bytes 8650752 | tf_op jit(solution)/shard_map/convert_element_type | solution.py:367
  5.5 0.0 copy-done
  5.5 0.0 copy-done.1
  5.5 6.4 %multiply_convert_fusion = (bf16[512,2816]{1,0:T(8,128)(2,1)}, bf16[512,2816]{1,0:T(8,128)(2,1)}) fusion(f32[512,2816]{1,0:T(8,128)S(1)} %copy-done, f32[512]{0:T(512)S(1)} %copy-done.1, f32[512,2816]{1,0:T(8,128)} %param.7), kind=kLoop, calls=%fused_computation | loop fusion | flops 5767168 | bytes 17303552 | tf_op jit(solution)/shard_map/convert_element_type | solution.py:366
  11.9 223.1 %shard_map.84 = (bf16[2,4096,1408]{2,1,0:T(8,128)(2,1)}, bf16[1408,4096]{1,0:T(8,128)(2,1)}, bf16[2,512,2816]{2,1,0:T(8,128)(2,1)}) custom-call(bf16[512,2816]{1,0:T(8,128)(2,1)} %get-tuple-element.19.wg, bf16[512,2816]{1,0:T(8,128)(2,1)} %get-tuple-element.18.wu, bf16[1408,1024]{1,0:T(8,128)(2,1)} %convert_element_type.11.d), custom_call_target="tpu_custom_call" | custom-call | tf_op jit(solution)/shard_map/pallas_call | solution.py:194
  235.1 21.3 %shard_map.85 = (bf16[4096,1408]{1,0:T(8,128)(2,1)}, bf16[4096,1408]{1,0:T(8,128)(2,1)}, bf16[192,1408]{1,0:T(8,128)(2,1)}) custom-call(bf16[192,4096]{1,0:T(8,128)(2,1)} %tok.1, bf16[2,4096,1408]{2,1,0:T(8,128)(2,1)} %get-tuple-element.11.both), custom_call_target="tpu_custom_call" | custom-call | tf_op jit(solution)/shard_map/pallas_call | solution.py:239
  256.4 12.6 %shard_map.86 = (bf16[1408,4096]{1,0:T(8,128)(2,1)}, bf16[8,192,512]{2,1,0:T(8,128)(2,1)}) custom-call(bf16[192,1408]{1,0:T(8,128)(2,1)} %get-tuple-element.14.hidden, bf16[1408,4096]{1,0:T(8,128)(2,1)} %get-tuple-element.15.down), custom_call_target="tpu_custom_call" | custom-call | tf_op jit(solution)/shard_map/pallas_call | solution.py:268
  269.0 30.4 %shard_map.87 = bf16[192,512]{1,0:T(8,128)(2,1)} custom-call(bf16[8,192,512]{2,1,0:T(8,128)(2,1)} %get-tuple-element.17.p), custom_call_target="tpu_custom_call" | custom-call | tf_op jit(solution)/shard_map/pallas_call | solution.py:331
  299.4 1.6 copy.10
Async XLA Ops:
  0.6 4.9 %copy-start = (f32[512,2816]{1,0:T(8,128)S(1)}, f32[512,2816]{1,0:T(8,128)}, u32[]{:S(2)}) copy-start(f32[512,2816]{1,0:T(8,128)} %param.8) | copy-start | bytes 17301508
  0.6 4.8 %copy-start.1 = (f32[512]{0:T(512)S(1)}, f32[512]{0:T(512)}, u32[]{:S(2)}) copy-start(f32[512]{0:T(512)} %param.6) | copy-start | bytes 6148
where the time goes:
time: 302 us; the launch traced here: 301 us
  Pallas kernels  287 us (95%)
  other arithmetic  11.3 us (4%)
    pallas_call x1, Pallas kernels, exchange(): pl.pallas_call(functools.partial(exchange_kernel, fs, tp, plan), out_shap...  223 us
    pallas_call x1, Pallas kernels, reduce_over_fs(): pl.pallas_call(functools.partial(reduce_kernel, fs), out_shape=jax.ShapeD...  30.4 us
    pallas_call x1, Pallas kernels, hidden_units(): pl.pallas_call(hidden_kernel, grid=(steps,), out_shape=(serving, serving,...  21.3 us
    pallas_call x1, Pallas kernels, partial_sums(): pl.pallas_call(partial_kernel, grid=(blocks,), out_shape=(jax.ShapeDtypeS...  12.6 us
    convert_element_type x1, other arithmetic, on_device(): up_cast = (up_trained * norm_gain[:, None]).astype(jnp.bfloat16)  6.43 us

commit v1 on v0

v1 whole, which is shorter than its diff:
```python
import functools

import jax
import jax.numpy as jnp
from jax import lax
from jax.experimental import pallas as pl
from jax.experimental.pallas import tpu as pltpu
from jax.sharding import PartitionSpec as P

MESH = pl.DeviceIdType.MESH
HOME, AWAY, BOTH = 0, 1, 2
LAYER_VMEM = 27 * 2 ** 20


SHARES = ((1, AWAY), (2, BOTH), (4, AWAY), (7, HOME), (6, BOTH), (6, BOTH), (6, BOTH))


def chunk_plan(rows):
    unit = max(16, rows // sum(share for share, _ in SHARES) // 16 * 16)
    plan, at = [], 0
    for i, (share, way) in enumerate(SHARES):
        size = rows - at if i == len(SHARES) - 1 else share * unit
        plan.append((at, size, way))
        at += size
    return tuple(plan)


def layer_kernel(fs, tp, plan, pieces, tok_hbm, gain, gate_f32, up_f32, down_f32,
                 out, dout, mixed, part, w, gcol, stage, dstage, tok, scale, nrm, acc, hidden,
                 pcross, pown, ybuf, sbuf, zbuf,
                 part_send, part_recv, own_send, relay_send, land_recv,
                 sib_send, sib_recv, cross_send, down_send, down_recv,
                 stage_sem, dstage_sem, tok_sem, keep_sem, ysend, yrecv, zsend, zrecv):
    f, t = lax.axis_index("fs"), lax.axis_index("tp")
    x, c = t // 2, lax.rem(t, 2)
    z, y = f // 2, lax.rem(f, 2)
    source_f32 = (gate_f32, up_f32)
    rows, wide = gate_f32.shape
    width = out.shape[2]
    units, dcols = down_f32.shape
    tokens = tok.shape[0]
    features = dout.shape[1]
    block_width = features // fs
    planes = fs // 2
    half = fs // 2
    sib, far = 2 * x + 1 - c, 2 * (1 - x) + c
    chunks = len(plan)
    slots = stage.shape[0]
    casts = [(k, g) for k in range(chunks) for g in range(2)]

    def fetch(i):
        k, g = casts[i]
        at, size, _ = plan[k]
        return pltpu.make_async_copy(
            source_f32[g].at[pl.ds(at, size), :], stage.at[i % slots, pl.ds(0, size), :], stage_sem.at[i % slots])

    depth = units // pieces

    def dfetch(i):
        return pltpu.make_async_copy(
            down_f32.at[pl.ds(i * depth, depth), :], dstage.at[i % 2], dstage_sem.at[i % 2])

    take_tok = pltpu.make_async_copy(tok_hbm, tok, tok_sem)
    for i in range(slots):
        fetch(i).start()
    for i in range(2):
        dfetch(i).start()
    take_tok.start()

    me = f * tp + t
    barrier = pltpu.get_barrier_semaphore()
    for i in range(1, fs * tp):
        other = lax.rem(me + i, fs * tp)
        pl.semaphore_signal(barrier, inc=1, device_id=(other // tp, lax.rem(other, tp)), device_id_type=MESH)
    gcol[...] = jnp.broadcast_to(gain[...], (128, rows)).T
    pl.semaphore_wait(barrier, fs * tp - 1)

    own_cross = z // 2 != x
    part_cross = z // 2 == x
    at_home = z // 2 == x
    true = f >= 0

    def uses(cross, way, dropped):
        return jnp.logical_not(cross) if way == dropped else true

    def remote(src, dst, ssem, rsem, fs_to, tp_to):
        return pltpu.make_async_remote_copy(
            src_ref=src, dst_ref=dst, send_sem=ssem, recv_sem=rsem,
            device_id=(fs_to, tp_to), device_id_type=MESH)

    sent = []

    def send(cond, copy):
        @pl.when(cond)
        def _():
            copy.start()
        sent.append((cond, copy))

    def to_serve(view, sems, k, cond, home, g):
        at, size, _ = plan[k]
        for yy in range(2):
            to = 2 * home + yy
            here = jnp.logical_and(to == f, c == g)
            send(jnp.logical_and(cond, jnp.logical_not(here)), remote(
                view(pl.ds(at, size), pl.ds(yy * width, width)),
                out.at[g, pl.ds(f * rows + at, size), :],
                sems.at[g, yy, k], land_recv.at[f, k], to, 2 * x + g))

    def part_copy(g, k):
        at, size, _ = plan[k]
        return remote(w.at[g, pl.ds(at, size), :], part.at[g, pl.ds(at, size), :],
                      part_send.at[g, k], part_recv.at[g, k], f, far)

    def give(i):
        k, g = casts[i]
        send(uses(own_cross, plan[k][2], HOME), part_copy(g, k))
        to_serve(lambda r, q: w.at[g, r, q], own_send, k, uses(own_cross, plan[k][2], AWAY), t, g)

    for i, (k, g) in enumerate(casts):
        at, size, _ = plan[k]
        fetch(i).wait()

        @pl.loop(0, size // 16)
        def _(r):
            r = pl.multiple_of(r * 16, 16)
            gains = gcol[pl.ds(at + r, 16), :]
            for j in range(wide // 128):
                lanes = pl.ds(j * 128, 128)
                w[g, pl.ds(at + r, 16), lanes] = (stage[i % slots, pl.ds(r, 16), lanes] * gains).astype(w.dtype)
        if i + slots < len(casts):
            fetch(i + slots).start()
        if i:
            give(i - 1)

    block = pl.ds(pl.multiple_of(t * dcols, dcols), dcols)
    for i in range(pieces):
        dfetch(i).wait()

        @pl.loop(0, depth // 16)
        def _(r):
            r = pl.multiple_of(r * 16, 16)
            dout[pl.ds(i * depth + r, 16), block] = dstage[i % 2, pl.ds(r, 16), :].astype(dout.dtype)
        if i + 2 < pieces:
            dfetch(i + 2).start()
        if i == 0:
            give(len(casts) - 1)

    take_tok.wait()
    step = 32

    @pl.loop(0, tokens // step)
    def _(i):
        some = pl.ds(pl.multiple_of(i * step, step), step)
        v = tok[some, :].astype(jnp.float32)
        scale[some, :] = lax.rsqrt(jnp.mean(v * v, axis=-1, keepdims=True) + 1e-06)

    down_far = remote(dout.at[:, block], dout.at[:, block], down_send.at[0], down_recv.at[0], f, far)
    down_sib = remote(dout.at[:, block], dout.at[:, block], down_send.at[1], down_recv.at[1], f, sib)
    send(true, down_far)
    send(true, down_sib)

    @pl.loop(0, fs)
    def _(s):
        v = tok[:, pl.ds(pl.multiple_of(s * rows, rows), rows)].astype(jnp.float32)
        v = (v * scale[...]).astype(nrm.dtype)
        for k, (at, size, _) in enumerate(plan):
            nrm[k, s, :, pl.ds(0, size)] = v[:, at:at + size]
    acc[...] = jnp.zeros_like(acc)

    for k in range(chunks):
        come = uses(part_cross, plan[k][2], HOME)

        @pl.when(come)
        def _():
            for g in range(2):
                part_copy(g, k).wait_recv()
        for g in range(2):
            to_serve(lambda r, q: part.at[g, r, q], relay_send, k, come, lax.rem(t + 2, tp), g)

    keeps = lax.rem(z, 2) == c
    mine = pl.ds(pl.multiple_of(f * rows, rows), rows)
    kept_copy = pltpu.make_async_copy(
        part.at[c, :, pl.ds(pl.multiple_of(y * width, 128), width)], out.at[c, mine, :], keep_sem)

    @pl.when(jnp.logical_and(keeps, jnp.logical_not(at_home)))
    def _():
        kept_copy.start()
        kept_copy.wait()

    @pl.when(jnp.logical_and(keeps, at_home))
    def _():
        @pl.loop(0, rows // 16)
        def _(r):
            r = pl.multiple_of(r * 16, 16)
            to = pl.multiple_of(f * rows + r, 16)
            out[c, pl.ds(to, 16), :] = w[c, pl.ds(r, 16), pl.ds(pl.multiple_of(y * width, 128), width)]

    def landed(g, k, source):
        at, size, _ = plan[k]
        return out.at[g, pl.ds(pl.multiple_of(source * rows + at, 16), size), :]

    def crossing(k, source):
        ref = landed(c, k, source)
        return remote(ref, ref, cross_send.at[source, k], land_recv.at[source, k], f, far)

    def beside(g, k, source):
        ref = landed(g, k, source)
        return remote(ref, ref, sib_send.at[source, k], sib_recv.at[source, k], f, sib)

    def arrive(k, source, cross):
        @pl.when(jnp.logical_not(jnp.logical_and(keeps, f == source)))
        def _():
            crossing(k, source).wait_recv()
        if cross:
            crossing(k, source).start()
        beside(c, k, source).start()

    def accumulate(k, source):
        at, size, _ = plan[k]
        beside(1 - c, k, source).wait_recv()
        left = nrm[k, source, :, pl.ds(0, size)]

        @pl.loop(0, 2)
        def _(g):
            acc[g] += jnp.dot(left, out[g, pl.ds(pl.multiple_of(source * rows + at, 16), size), :],
                              preferred_element_type=jnp.float32)

    same = (f // half) * half
    turned = half - same

    def side(k):
        return at_home if plan[k][2] == HOME else jnp.logical_not(at_home)

    one_way = [k for k in range(chunks) if plan[k][2] != BOTH]
    both_ways = [k for k in range(chunks) if plan[k][2] == BOTH]
    for k in one_way:
        @pl.when(side(k))
        def _():
            @pl.loop(0, half)
            def _(i):
                arrive(k, turned + i, True)
    for k in one_way:
        @pl.loop(0, half)
        def _(i):
            arrive(k, same + i, False)
    due = [(k, same, half) for k in one_way]
    for k in both_ways:
        if k == both_ways[-1]:
            down_far.wait_recv()
            fblock = pl.ds(pl.multiple_of(far * dcols, dcols), dcols)
            send(true, remote(dout.at[:, fblock], dout.at[:, fblock], down_send.at[2], down_recv.at[2], f, sib))

        @pl.loop(0, fs)
        def _(i):
            arrive(k, i, False)
        for kk, base, count in due:
            @pl.loop(0, count)
            def _(i):
                accumulate(kk, base + i)
        due = [(k, 0, fs)]
    for k in one_way:
        @pl.when(jnp.logical_not(side(k)))
        def _():
            @pl.loop(0, half)
            def _(i):
                arrive(k, turned + i, False)
    for kk, base, count in due + [(k, turned, half) for k in one_way]:
        @pl.loop(0, count)
        def _(i):
            accumulate(kk, base + i)

    hidden[...] = (jax.nn.silu(acc[0]) * acc[1]).astype(hidden.dtype)
    down_sib.wait_recv()
    remote(dout.at[:, block], dout.at[:, block], down_send.at[2], down_recv.at[2], f, sib).wait_recv()

    def sums(to):
        at = pl.multiple_of(to * block_width, block_width)
        return jnp.dot(hidden[...], dout[:, pl.ds(at, block_width)], preferred_element_type=jnp.float32)

    order = sorted(range(1, planes), key=lambda o: abs(o - planes // 2)) + [0]
    across = {off: remote(pcross.at[off], ybuf.at[off], ysend.at[off], yrecv.at[off], 2 * z + 1 - y, t) for off in order}
    last = None
    for off in order:
        pcross[off] = sums(2 * lax.rem(z + off, planes) + 1 - y).astype(pcross.dtype)
        if last is not None:
            across[last].start()
        last = off
    for i, off in enumerate(order):
        pown[off] = sums(2 * lax.rem(z + off, planes) + y)
        if i == 0:
            across[last].start()
    along = {}
    total = None
    for off in order:
        to = lax.rem(z + off, planes)
        across[off].wait_recv()
        pair = pown[off] + ybuf[off].astype(jnp.float32)
        if off:
            sbuf[off] = pair.astype(sbuf.dtype)
            along[off] = remote(sbuf.at[off], zbuf.at[off], zsend.at[off], zrecv.at[off], 2 * to + y, t)
            along[off].start()
        else:
            total = pair
    for off in order[:-1]:
        along[off].wait_recv()
        total += zbuf[off].astype(jnp.float32)
    mixed[...] = total.astype(mixed.dtype)

    for off in order:
        across[off].wait_send()
        if off:
            along[off].wait_send()
    for cond, copy in sent:
        @pl.when(cond)
        def _():
            copy.wait_send()
    for k in range(chunks):
        @pl.loop(0, fs)
        def _(i):
            beside(c, k, i).wait_send()
        if plan[k][2] != BOTH:
            @pl.when(side(k))
            def _():
                @pl.loop(0, half)
                def _(i):
                    crossing(k, turned + i).wait_send()


def layer(tok, gain, gate, up, down, fs, tp):
    rows, wide = gate.shape
    width = wide * tp // fs
    units, dcols = down.shape
    features = dcols * tp
    tokens = tok.shape[0]
    block_width = features // fs
    plan = chunk_plan(rows)
    n = len(plan)
    widest = max(size for _, size, _ in plan)
    pieces = 8
    bf16 = jnp.bfloat16
    dma = pltpu.SemaphoreType.DMA
    hbm = pl.BlockSpec(memory_space=pltpu.HBM)
    vmem = pl.BlockSpec(memory_space=pltpu.VMEM)
    slots = pltpu.VMEM((fs // 2, tokens, block_width), bf16)
    return pl.pallas_call(
        functools.partial(layer_kernel, fs, tp, plan, pieces),
        out_shape=(
            pltpu.VMEM((2, rows * fs, width), bf16),
            pltpu.VMEM((units, features), bf16),
            pltpu.VMEM((tokens, block_width), bf16),
            pltpu.HBM((2, rows, wide), bf16),
        ),
        in_specs=[hbm, vmem, hbm, hbm, hbm],
        out_specs=(vmem, vmem, vmem, hbm),
        scratch_shapes=[
            pltpu.VMEM((2, rows, wide), bf16),
            pltpu.VMEM((rows, 128), jnp.float32),
            pltpu.VMEM((3, widest, wide), jnp.float32),
            pltpu.VMEM((2, units // pieces, dcols), jnp.float32),
            pltpu.VMEM(tok.shape, bf16),
            pltpu.VMEM((tokens, 1), jnp.float32),
            pltpu.VMEM((n, fs, tokens, 128), bf16),
            pltpu.VMEM((2, tokens, width), jnp.float32),
            pltpu.VMEM((tokens, width), bf16),
            slots, pltpu.VMEM((fs // 2, tokens, block_width), jnp.float32), slots, slots, slots,
            dma((2, n)), dma((2, n)), dma((2, 2, n)), dma((2, 2, n)), dma((fs, n)),
            dma((fs, n)), dma((fs, n)), dma((fs, n)), dma((3,)), dma((3,)),
            dma((3,)), dma((2,)), dma, dma,
            dma((fs // 2,)), dma((fs // 2,)), dma((fs // 2,)), dma((fs // 2,)),
        ],
        compiler_params=pltpu.CompilerParams(
            collective_id=0, has_side_effects=True, vmem_limit_bytes=LAYER_VMEM),
    )(tok, gain, gate, up, down)


def deliver_kernel(pairs, *refs):
    srcs, dsts, sems = refs[:pairs[-1][0] + 1], refs[pairs[-1][0] + 1:-1], refs[-1]
    copies = []
    for (i, view, cuts), dst in zip(pairs, dsts):
        src = srcs[i] if view is None else srcs[i].at[view]
        depth = dst.shape[0] // cuts
        copies += [(src.at[pl.ds(k * depth, depth)], dst.at[pl.ds(k * depth, depth)]) for k in range(cuts)]
    copies = [pltpu.make_async_copy(src, dst, sems.at[i]) for i, (src, dst) in enumerate(copies)]
    for copy in copies:
        copy.start()
    for copy in copies:
        copy.wait()


def deliver(srcs, pairs):
    def shape(i, view):
        return srcs[i].shape if view is None else srcs[i].shape[1:]

    return pl.pallas_call(
        functools.partial(deliver_kernel, pairs),
        out_shape=tuple(pltpu.HBM(shape(i, view), srcs[i].dtype) for i, view, _ in pairs),
        in_specs=[pl.BlockSpec(memory_space=pltpu.VMEM)] * len(srcs),
        out_specs=(pl.BlockSpec(memory_space=pltpu.HBM),) * len(pairs),
        scratch_shapes=[pltpu.SemaphoreType.DMA((sum(cuts for _, _, cuts in pairs),))],
        compiler_params=pltpu.CompilerParams(vmem_limit_bytes=2 ** 20),
    )(*srcs)


def by_kernels(prompt_tokens, norm_gain, gate_trained, up_trained, down_trained):
    fs, tp = lax.axis_size("fs"), lax.axis_size("tp")
    both, down, mixed, _ = layer(
        prompt_tokens, norm_gain[None, :], gate_trained, up_trained, down_trained, fs, tp)
    gate_serving, up_serving = deliver((both,), ((0, 0, 8), (0, 1, 8)))
    down_serving, mixed = deliver((down, mixed), ((0, None, 8), (1, None, 1)))
    return gate_serving, up_serving, down_serving, mixed


def gather_by_collectives(gate_cast, up_cast, down_cast):
    fs_count = lax.axis_size("fs")
    down_serving = lax.all_gather(down_cast, "tp", axis=1, tiled=True)

    def serve(cast):
        part = lax.all_to_all(cast, "tp", split_axis=0, concat_axis=1, tiled=True)
        mid = lax.all_to_all(part, "fs", split_axis=1, concat_axis=0, tiled=True)
        share, width = mid.shape[0] // fs_count, mid.shape[1]
        blocks = lax.all_gather(mid.reshape(fs_count, share, width), "tp", axis=1, tiled=True)
        return blocks.reshape(-1, width)

    return serve(gate_cast), serve(up_cast), down_serving


def on_device(prompt_tokens, norm_gain, gate_trained, up_trained, down_trained):
    fs, tp = lax.axis_size("fs"), lax.axis_size("tp")
    routed = fs == 2 * tp and tp == 4
    if routed:
        return by_kernels(prompt_tokens, norm_gain, gate_trained, up_trained, down_trained)
    gate_cast = (gate_trained * norm_gain[:, None]).astype(jnp.bfloat16)
    up_cast = (up_trained * norm_gain[:, None]).astype(jnp.bfloat16)
    down_cast = down_trained.astype(jnp.bfloat16)
    gate_serving, up_serving, down_serving = gather_by_collectives(gate_cast, up_cast, down_cast)
    tokens = prompt_tokens.astype(jnp.float32)
    scale = lax.rsqrt(jnp.mean(tokens * tokens, axis=-1, keepdims=True) + 1e-06)
    normed = (tokens * scale).astype(jnp.bfloat16)
    contract = (((0,), (1,)), ((), ()))
    gate_cols = lax.dot_general(gate_serving, normed, contract, preferred_element_type=jnp.float32)
    up_cols = lax.dot_general(up_serving, normed, contract, preferred_element_type=jnp.float32)
    hidden_cols = (jax.nn.silu(gate_cols) * up_cols).astype(jnp.bfloat16)
    summed = lax.psum_scatter(
        lax.dot_general(
            down_serving, hidden_cols, (((0,), (0,)), ((), ())), preferred_element_type=jnp.float32
        ),
        "fs",
        scatter_dimension=0,
        tiled=True,
    )
    mixed = summed.T.astype(jnp.bfloat16)
    return (gate_serving, up_serving, down_serving, mixed)


def solution(mesh):
    return jax.shard_map(
        on_device,
        mesh=mesh,
        in_specs=(P("tp", None), P("fs"), P("fs", "tp"), P("fs", "tp"), P("fs", "tp")),
        out_specs=(P(None, "fs"), P(None, "fs"), P("fs", None), P("tp", "fs")),
        check_vma=False,
    )
```

time: 302 us -> 275 us (0.911)
  Pallas kernels: 287 us -> 274 us
  other arithmetic: 11.3 us -> 0 us
    pallas_call x4 -> x3, Pallas kernels: 287 us -> 274 us  [the longest x1 262 us: layer(): pl.pallas_call(functools.partial(layer_kernel, fs, tp, plan, pieces), out...]
    convert_element_type x2 -> x0, other arithmetic: 11.3 us -> none  [the longest x1 6.43 us: on_device(): up_cast = (up_trained * norm_gain[:, None]).astype(jnp.bfloat16)]
where the time goes in v1:
time: 275 us; the launch traced here: 274 us
  Pallas kernels  274 us (100%)
    pallas_call x1, Pallas kernels, layer(): pl.pallas_call(functools.partial(layer_kernel, fs, tp, plan, pieces), out...  262 us
    pallas_call x2, Pallas kernels, deliver(): pl.pallas_call(functools.partial(deliver_kernel, pairs), out_shape=tuple(...  12.2 us

profile of v1, /device:TPU:0, one launch (start us, length us, event | category | flops | bytes accessed | tf_op | source)
XLA Modules:
  0.0 274.4 jit_solution(10127778469228034067)
XLA Ops:
  0.6 261.5 %shard_map.84 = (bf16[2,4096,1408]{2,1,0:T(8,128)(2,1)S(1)}, bf16[1408,4096]{1,0:T(8,128)(2,1)S(1)}, bf16[192,512]{1,0:T(8,128)(2,1)S(1)}, bf16[2,512,2816]{2,1,0:T(8,128)(2,1)}) custom-call(bf16[192,4096]{1,0:T(8,128)(2,1)} %tok_hbm.1, f32[1,512]{1,0:T(1,128)} %bitcast.1, f32[512,2816]{1,0:T(8,128)} %gate_f32.1, f32[512,2816]{1,0:T(8,128)} %up_f32.1, ...), custom_call_target="tpu_custom_call" | custom-call | tf_op jit(solution)/shard_map/pallas_call | solution.py:345
  262.2 7.9 %shard_map.85 = (bf16[4096,1408]{1,0:T(8,128)(2,1)}, bf16[4096,1408]{1,0:T(8,128)(2,1)}) custom-call(bf16[2,4096,1408]{2,1,0:T(8,128)(2,1)S(1)} %get-tuple-element.11.refs_0_), custom_call_target="tpu_custom_call" | custom-call | tf_op jit(solution)/shard_map/pallas_call | solution.py:394
  270.0 4.3 %shard_map.86 = (bf16[1408,4096]{1,0:T(8,128)(2,1)}, bf16[192,512]{1,0:T(8,128)(2,1)}) custom-call(bf16[1408,4096]{1,0:T(8,128)(2,1)S(1)} %get-tuple-element.14.refs_0_, bf16[192,512]{1,0:T(8,128)(2,1)S(1)} %get-tuple-element.15.refs_1_), custom_call_target="tpu_custom_call" | custom-call | tf_op jit(solution)/shard_map/pallas_call | solution.py:394

commit v2 on v1

--- a/solution.py
+++ b/solution.py
@@ -10,26 +10,39 @@
 MESH = pl.DeviceIdType.MESH
 HOME, AWAY, BOTH = 0, 1, 2
 LAYER_VMEM = 27 * 2 ** 20
-
-
-SHARES = ((1, AWAY), (2, BOTH), (4, AWAY), (7, HOME), (6, BOTH), (6, BOTH), (6, BOTH))
+EARLY_RELAY = 8
+
+
+SHARES = ((1, AWAY), (2, BOTH), (4, AWAY), (7, HOME), (2, AWAY), (5, BOTH), (4, BOTH), (4, BOTH), (3, BOTH))
+DOWN_CUTS = 8
+HALVES = 2
 
 
 def chunk_plan(rows):
     unit = max(16, rows // sum(share for share, _ in SHARES) // 16 * 16)
-    plan, at = [], 0
-    for i, (share, way) in enumerate(SHARES):
-        size = rows - at if i == len(SHARES) - 1 else share * unit
-        plan.append((at, size, way))
-        at += size
+    sizes = [share * unit for share, _ in SHARES]
+    sizes[-1] += rows - sum(sizes)
+    at, plan = 0, [None] * len(SHARES)
+    for both in (False, True):
+        for i, (_, way) in enumerate(SHARES):
+            if (way == BOTH) == both:
+                plan[i] = (at, sizes[i], way)
+                at += sizes[i]
     return tuple(plan)
+
+
+def groups_of(plan):
+    one_way = [k for k, (_, _, way) in enumerate(plan) if way != BOTH]
+    both_ways = [k for k, (_, _, way) in enumerate(plan) if way == BOTH]
+    middle = len(both_ways) // 2
+    return one_way, both_ways[:middle], both_ways[middle:]
 
 
 def layer_kernel(fs, tp, plan, pieces, tok_hbm, gain, gate_f32, up_f32, down_f32,
                  out, dout, mixed, part, w, gcol, stage, dstage, tok, scale, nrm, acc, hidden,
                  pcross, pown, ybuf, sbuf, zbuf,
                  part_send, part_recv, own_send, relay_send, land_recv,
-                 sib_send, sib_recv, cross_send, down_send, down_recv,
+                 sib_send, sib_recv, cross_send, down_send, down_recv, sibling_send, sibling_recv,
                  stage_sem, dstage_sem, tok_sem, keep_sem, ysend, yrecv, zsend, zrecv):
     f, t = lax.axis_index("fs"), lax.axis_index("tp")
     x, c = t // 2, lax.rem(t, 2)
@@ -46,6 +59,8 @@
     sib, far = 2 * x + 1 - c, 2 * (1 - x) + c
     chunks = len(plan)
     slots = stage.shape[0]
+    groups = groups_of(plan)
+    spans = [(plan[group[0]][0], sum(plan[k][1] for k in group)) for group in groups]
     casts = [(k, g) for k in range(chunks) for g in range(2)]
 
     def fetch(i):
@@ -114,7 +129,20 @@
     def give(i):
         k, g = casts[i]
         send(uses(own_cross, plan[k][2], HOME), part_copy(g, k))
-        to_serve(lambda r, q: w.at[g, r, q], own_send, k, uses(own_cross, plan[k][2], AWAY), t, g)
+        if plan[k][2] != AWAY:
+            to_serve(lambda r, q: w.at[g, r, q], own_send, k, own_cross, t, g)
+
+    def relay(k):
+        come = uses(part_cross, plan[k][2], HOME)
+
+        @pl.when(come)
+        def _():
+            for g in range(2):
+                part_copy(g, k).wait_recv()
+        for g in range(2):
+            to_serve(lambda r, q: part.at[g, r, q], relay_send, k, come, lax.rem(t + 2, tp), g)
+        for g in range(2):
+            to_serve(lambda r, q: w.at[g, r, q], own_send, k, at_home, t, g)
 
     for i, (k, g) in enumerate(casts):
         at, size, _ = plan[k]
@@ -131,6 +159,8 @@
             fetch(i + slots).start()
         if i:
             give(i - 1)
+        if i == EARLY_RELAY:
+            relay(0)
 
     block = pl.ds(pl.multiple_of(t * dcols, dcols), dcols)
     for i in range(pieces):
@@ -154,28 +184,33 @@
         v = tok[some, :].astype(jnp.float32)
         scale[some, :] = lax.rsqrt(jnp.mean(v * v, axis=-1, keepdims=True) + 1e-06)
 
-    down_far = remote(dout.at[:, block], dout.at[:, block], down_send.at[0], down_recv.at[0], f, far)
-    down_sib = remote(dout.at[:, block], dout.at[:, block], down_send.at[1], down_recv.at[1], f, sib)
-    send(true, down_far)
+    relay(1)
+    fblock = pl.ds(pl.multiple_of(far * dcols, dcols), dcols)
+    cut = units // DOWN_CUTS
+
+    def down_far(i):
+        ref = dout.at[pl.ds(i * cut, cut), block]
+        return remote(ref, ref, down_send.at[0, i], down_recv.at[0, i], f, far)
+
+    def down_on(i):
+        ref = dout.at[pl.ds(i * cut, cut), fblock]
+        return remote(ref, ref, down_send.at[1, i], down_recv.at[1, i], f, sib)
+
+    down_sib = remote(dout.at[:, block], dout.at[:, block], sibling_send, sibling_recv, f, sib)
+    for i in range(DOWN_CUTS):
+        send(jnp.logical_not(at_home), down_far(i))
     send(true, down_sib)
 
     @pl.loop(0, fs)
     def _(s):
         v = tok[:, pl.ds(pl.multiple_of(s * rows, rows), rows)].astype(jnp.float32)
         v = (v * scale[...]).astype(nrm.dtype)
-        for k, (at, size, _) in enumerate(plan):
-            nrm[k, s, :, pl.ds(0, size)] = v[:, at:at + size]
+        for j, (at, size) in enumerate(spans):
+            nrm[j, s, :, pl.ds(0, size)] = v[:, at:at + size]
     acc[...] = jnp.zeros_like(acc)
 
-    for k in range(chunks):
-        come = uses(part_cross, plan[k][2], HOME)
-
-        @pl.when(come)
-        def _():
-            for g in range(2):
-                part_copy(g, k).wait_recv()
-        for g in range(2):
-            to_serve(lambda r, q: part.at[g, r, q], relay_send, k, come, lax.rem(t + 2, tp), g)
+    for k in range(2, chunks):
+        relay(k)
 
     keeps = lax.rem(z, 2) == c
     mine = pl.ds(pl.multiple_of(f * rows, rows), rows)
@@ -215,10 +250,11 @@
             crossing(k, source).start()
         beside(c, k, source).start()
 
-    def accumulate(k, source):
-        at, size, _ = plan[k]
-        beside(1 - c, k, source).wait_recv()
-        left = nrm[k, source, :, pl.ds(0, size)]
+    def accumulate(j, source):
+        at, size = spans[j]
+        for k in groups[j]:
+            beside(1 - c, k, source).wait_recv()
+        left = nrm[j, source, :, pl.ds(0, size)]
 
         @pl.loop(0, 2)
         def _(g):
@@ -231,85 +267,139 @@
     def side(k):
         return at_home if plan[k][2] == HOME else jnp.logical_not(at_home)
 
-    one_way = [k for k in range(chunks) if plan[k][2] != BOTH]
-    both_ways = [k for k in range(chunks) if plan[k][2] == BOTH]
+    def pass_on(cond, cuts):
+        for i in cuts:
+            @pl.when(cond)
+            def _():
+                down_far(i).wait_recv()
+            send(cond, down_on(i))
+
+    one_way, early, late = groups
     for k in one_way:
         @pl.when(side(k))
         def _():
             @pl.loop(0, half)
             def _(i):
                 arrive(k, turned + i, True)
+    for i in range(DOWN_CUTS):
+        send(at_home, down_far(i))
     for k in one_way:
         @pl.loop(0, half)
         def _(i):
             arrive(k, same + i, False)
-    due = [(k, same, half) for k in one_way]
-    for k in both_ways:
-        if k == both_ways[-1]:
-            down_far.wait_recv()
-            fblock = pl.ds(pl.multiple_of(far * dcols, dcols), dcols)
-            send(true, remote(dout.at[:, fblock], dout.at[:, fblock], down_send.at[2], down_recv.at[2], f, sib))
-
+    for k in early:
         @pl.loop(0, fs)
         def _(i):
             arrive(k, i, False)
-        for kk, base, count in due:
-            @pl.loop(0, count)
+
+    @pl.loop(0, half)
+    def _(i):
+        accumulate(0, same + i)
+    for k in late[:-1]:
+        @pl.loop(0, fs)
+        def _(i):
+            arrive(k, i, False)
+        if k == late[0]:
+            @pl.loop(0, fs)
             def _(i):
-                accumulate(kk, base + i)
-        due = [(k, 0, fs)]
+                accumulate(1, i)
+    pass_on(at_home, range(DOWN_CUTS))
+    pass_on(jnp.logical_not(at_home), range(DOWN_CUTS // 2))
     for k in one_way:
         @pl.when(jnp.logical_not(side(k)))
         def _():
             @pl.loop(0, half)
             def _(i):
                 arrive(k, turned + i, False)
-    for kk, base, count in due + [(k, turned, half) for k in one_way]:
-        @pl.loop(0, count)
-        def _(i):
-            accumulate(kk, base + i)
+
+    @pl.loop(0, half)
+    def _(i):
+        arrive(late[-1], same + i, False)
+        accumulate(0, turned + i)
+
+    @pl.loop(0, half)
+    def _(i):
+        arrive(late[-1], turned + i, False)
+        accumulate(2, same + i)
+
+    @pl.loop(0, half)
+    def _(i):
+        accumulate(2, turned + i)
 
     hidden[...] = (jax.nn.silu(acc[0]) * acc[1]).astype(hidden.dtype)
     down_sib.wait_recv()
-    remote(dout.at[:, block], dout.at[:, block], down_send.at[2], down_recv.at[2], f, sib).wait_recv()
 
     def sums(to):
         at = pl.multiple_of(to * block_width, block_width)
         return jnp.dot(hidden[...], dout[:, pl.ds(at, block_width)], preferred_element_type=jnp.float32)
 
-    order = sorted(range(1, planes), key=lambda o: abs(o - planes // 2)) + [0]
-    across = {off: remote(pcross.at[off], ybuf.at[off], ysend.at[off], yrecv.at[off], 2 * z + 1 - y, t) for off in order}
-    last = None
-    for off in order:
-        pcross[off] = sums(2 * lax.rem(z + off, planes) + 1 - y).astype(pcross.dtype)
-        if last is not None:
-            across[last].start()
-        last = off
-    for i, off in enumerate(order):
-        pown[off] = sums(2 * lax.rem(z + off, planes) + y)
-        if i == 0:
-            across[last].start()
-    along = {}
-    total = None
-    for off in order:
-        to = lax.rem(z + off, planes)
-        across[off].wait_recv()
-        pair = pown[off] + ybuf[off].astype(jnp.float32)
-        if off:
-            sbuf[off] = pair.astype(sbuf.dtype)
-            along[off] = remote(sbuf.at[off], zbuf.at[off], zsend.at[off], zrecv.at[off], 2 * to + y, t)
-            along[off].start()
-        else:
-            total = pair
-    for off in order[:-1]:
-        along[off].wait_recv()
-        total += zbuf[off].astype(jnp.float32)
+    order = (3, 2, 1, 0)
+    level = {3: 3 - z, 2: lax.rem(z + 2, 4), 1: z + 1 - 2 * lax.rem(z, 2), 0: z}
+    def collect(cond):
+        @pl.when(cond)
+        def _():
+            for i in range(DOWN_CUTS):
+                down_on(i).wait_recv()
+
+    share = tokens // HALVES
+    halves = [pl.ds(h * share, share) for h in range(HALVES)]
+
+    def across(m, h):
+        return remote(pcross.at[m, halves[h]], ybuf.at[m, halves[h]], ysend.at[m, h], yrecv.at[m, h], 2 * z + 1 - y, t)
+
+    def along(m, h):
+        return remote(sbuf.at[m, halves[h]], zbuf.at[m, halves[h]], zsend.at[m, h], zrecv.at[m, h], 2 * level[m] + y, t)
+
+    def theirs(m):
+        pcross[m] = sums(2 * level[m] + 1 - y).astype(pcross.dtype)
+
+    def ours(m):
+        pown[m] = sums(2 * level[m] + y)
+
+    def offer(m):
+        for h in range(HALVES):
+            across(m, h).start()
+
+    def pair(m):
+        for h, some in enumerate(halves):
+            across(m, h).wait_recv()
+            total = pown[m, some] + ybuf[m, some].astype(jnp.float32)
+            if m:
+                sbuf[m, some] = total.astype(sbuf.dtype)
+                along(m, h).start()
+            else:
+                pown[m, some] = total
+
+    collect(at_home)
+    theirs(3)
+    theirs(2)
+    offer(3)
+    ours(3)
+    offer(2)
+    ours(2)
+    pair(3)
+    pass_on(jnp.logical_not(at_home), range(DOWN_CUTS // 2, DOWN_CUTS))
+    collect(jnp.logical_not(at_home))
+    theirs(1)
+    theirs(0)
+    offer(1)
+    ours(1)
+    offer(0)
+    ours(0)
+    for m in (2, 1, 0):
+        pair(m)
+    total = pown[0]
+    for m in (1, 3, 2):
+        for h in range(HALVES):
+            along(m, h).wait_recv()
+        total += zbuf[m].astype(jnp.float32)
     mixed[...] = total.astype(mixed.dtype)
 
-    for off in order:
-        across[off].wait_send()
-        if off:
-            along[off].wait_send()
+    for m in order:
+        for h in range(HALVES):
+            across(m, h).wait_send()
+            if m:
+                along(m, h).wait_send()
     for cond, copy in sent:
         @pl.when(cond)
         def _():
@@ -337,6 +427,7 @@
     n = len(plan)
     widest = max(size for _, size, _ in plan)
     pieces = 8
+    deepest = max(-(-sum(plan[k][1] for k in group) // 128) * 128 for group in groups_of(plan))
     bf16 = jnp.bfloat16
     dma = pltpu.SemaphoreType.DMA
     hbm = pl.BlockSpec(memory_space=pltpu.HBM)
@@ -359,14 +450,14 @@
             pltpu.VMEM((2, units // pieces, dcols), jnp.float32),
             pltpu.VMEM(tok.shape, bf16),
             pltpu.VMEM((tokens, 1), jnp.float32),
-            pltpu.VMEM((n, fs, tokens, 128), bf16),
+            pltpu.VMEM((3, fs, tokens, deepest), bf16),
             pltpu.VMEM((2, tokens, width), jnp.float32),
             pltpu.VMEM((tokens, width), bf16),
             slots, pltpu.VMEM((fs // 2, tokens, block_width), jnp.float32), slots, slots, slots,
             dma((2, n)), dma((2, n)), dma((2, 2, n)), dma((2, 2, n)), dma((fs, n)),
-            dma((fs, n)), dma((fs, n)), dma((fs, n)), dma((3,)), dma((3,)),
+            dma((fs, n)), dma((fs, n)), dma((fs, n)), dma((2, DOWN_CUTS)), dma((2, DOWN_CUTS)), dma, dma,
             dma((3,)), dma((2,)), dma, dma,
-            dma((fs // 2,)), dma((fs // 2,)), dma((fs // 2,)), dma((fs // 2,)),
+            dma((fs // 2, HALVES)), dma((fs // 2, HALVES)), dma((fs // 2, HALVES)), dma((fs // 2, HALVES)),
         ],
         compiler_params=pltpu.CompilerParams(
             collective_id=0, has_side_effects=True, vmem_limit_bytes=LAYER_VMEM),

time: 275 us -> 253 us (0.920)
  Pallas kernels: 274 us -> 252 us
    pallas_call x1, Pallas kernels: 262 us -> 240 us  [layer(): pl.pallas_call(functools.partial(layer_kernel, fs, tp, plan, pieces), out...]
where the time goes in v2:
time: 253 us
  Pallas kernels  252 us (100%)
    pallas_call x1, Pallas kernels, layer(): pl.pallas_call(functools.partial(layer_kernel, fs, tp, plan, pieces), out...  240 us
    pallas_call x2, Pallas kernels, deliver(): pl.pallas_call(functools.partial(deliver_kernel, pairs), out_shape=tuple(...  12.2 us

profile of v2, /device:TPU:0, one launch (start us, length us, event | category | flops | bytes accessed | tf_op | source)
XLA Modules:
  0.0 252.5 jit_solution(8663073584862458858)
XLA Ops:
  0.6 239.7 %shard_map.84 = (bf16[2,4096,1408]{2,1,0:T(8,128)(2,1)S(1)}, bf16[1408,4096]{1,0:T(8,128)(2,1)S(1)}, bf16[192,512]{1,0:T(8,128)(2,1)S(1)}, bf16[2,512,2816]{2,1,0:T(8,128)(2,1)}) custom-call(bf16[192,4096]{1,0:T(8,128)(2,1)} %tok_hbm.1, f32[1,512]{1,0:T(1,128)} %bitcast.1, f32[512,2816]{1,0:T(8,128)} %gate_f32.1, f32[512,2816]{1,0:T(8,128)} %up_f32.1, ...), custom_call_target="tpu_custom_call" | custom-call | tf_op jit(solution)/shard_map/pallas_call | solution.py:436
  240.3 7.9 %shard_map.85 = (bf16[4096,1408]{1,0:T(8,128)(2,1)}, bf16[4096,1408]{1,0:T(8,128)(2,1)}) custom-call(bf16[2,4096,1408]{2,1,0:T(8,128)(2,1)S(1)} %get-tuple-element.11.refs_0_), custom_call_target="tpu_custom_call" | custom-call | tf_op jit(solution)/shard_map/pallas_call | solution.py:485
  248.2 4.3 %shard_map.86 = (bf16[1408,4096]{1,0:T(8,128)(2,1)}, bf16[192,512]{1,0:T(8,128)(2,1)}) custom-call(bf16[1408,4096]{1,0:T(8,128)(2,1)S(1)} %get-tuple-element.14.refs_0_, bf16[192,512]{1,0:T(8,128)(2,1)S(1)} %get-tuple-element.15.refs_1_), custom_call_target="tpu_custom_call" | custom-call | tf_op jit(solution)/shard_map/pallas_call | solution.py:485

commit v3 on v2

--- a/solution.py
+++ b/solution.py
@@ -11,9 +11,10 @@
 HOME, AWAY, BOTH = 0, 1, 2
 LAYER_VMEM = 27 * 2 ** 20
 EARLY_RELAY = 8
-
-
-SHARES = ((1, AWAY), (2, BOTH), (4, AWAY), (7, HOME), (2, AWAY), (5, BOTH), (4, BOTH), (4, BOTH), (3, BOTH))
+EARLY_CASTS = 2
+
+
+SHARES = ((1, AWAY), (2, BOTH), (4, AWAY), (7, HOME), (2, AWAY), (6, BOTH), (6, BOTH), (4, BOTH))
 DOWN_CUTS = 8
 HALVES = 2
 
@@ -88,7 +89,6 @@
         other = lax.rem(me + i, fs * tp)
         pl.semaphore_signal(barrier, inc=1, device_id=(other // tp, lax.rem(other, tp)), device_id_type=MESH)
     gcol[...] = jnp.broadcast_to(gain[...], (128, rows)).T
-    pl.semaphore_wait(barrier, fs * tp - 1)
 
     own_cross = z // 2 != x
     part_cross = z // 2 == x
@@ -126,25 +126,8 @@
         return remote(w.at[g, pl.ds(at, size), :], part.at[g, pl.ds(at, size), :],
                       part_send.at[g, k], part_recv.at[g, k], f, far)
 
-    def give(i):
+    def cast(i):
         k, g = casts[i]
-        send(uses(own_cross, plan[k][2], HOME), part_copy(g, k))
-        if plan[k][2] != AWAY:
-            to_serve(lambda r, q: w.at[g, r, q], own_send, k, own_cross, t, g)
-
-    def relay(k):
-        come = uses(part_cross, plan[k][2], HOME)
-
-        @pl.when(come)
-        def _():
-            for g in range(2):
-                part_copy(g, k).wait_recv()
-        for g in range(2):
-            to_serve(lambda r, q: part.at[g, r, q], relay_send, k, come, lax.rem(t + 2, tp), g)
-        for g in range(2):
-            to_serve(lambda r, q: w.at[g, r, q], own_send, k, at_home, t, g)
-
-    for i, (k, g) in enumerate(casts):
         at, size, _ = plan[k]
         fetch(i).wait()
 
@@ -157,8 +140,33 @@
                 w[g, pl.ds(at + r, 16), lanes] = (stage[i % slots, pl.ds(r, 16), lanes] * gains).astype(w.dtype)
         if i + slots < len(casts):
             fetch(i + slots).start()
-        if i:
-            give(i - 1)
+
+    def give(i):
+        k, g = casts[i]
+        send(uses(own_cross, plan[k][2], HOME), part_copy(g, k))
+        if plan[k][2] != AWAY:
+            to_serve(lambda r, q: w.at[g, r, q], own_send, k, own_cross, t, g)
+
+    def relay(k):
+        come = uses(part_cross, plan[k][2], HOME)
+
+        @pl.when(come)
+        def _():
+            for g in range(2):
+                part_copy(g, k).wait_recv()
+        for g in range(2):
+            to_serve(lambda r, q: part.at[g, r, q], relay_send, k, come, lax.rem(t + 2, tp), g)
+        for g in range(2):
+            to_serve(lambda r, q: w.at[g, r, q], own_send, k, at_home, t, g)
+
+    for i in range(EARLY_CASTS):
+        cast(i)
+    pl.semaphore_wait(barrier, fs * tp - 1)
+    for i in range(EARLY_CASTS - 1):
+        give(i)
+    for i in range(EARLY_CASTS, len(casts)):
+        cast(i)
+        give(i - 1)
         if i == EARLY_RELAY:
             relay(0)
 
@@ -185,15 +193,18 @@
         scale[some, :] = lax.rsqrt(jnp.mean(v * v, axis=-1, keepdims=True) + 1e-06)
 
     relay(1)
-    fblock = pl.ds(pl.multiple_of(far * dcols, dcols), dcols)
-    cut = units // DOWN_CUTS
+    cut = features // fs * 2 // DOWN_CUTS
+
+    def down_cut(home, i):
+        at = home * dcols + i % 2 * block_width + i // 2 * cut
+        return dout.at[:, pl.ds(pl.multiple_of(at, 128), cut)]
 
     def down_far(i):
-        ref = dout.at[pl.ds(i * cut, cut), block]
+        ref = down_cut(t, i)
         return remote(ref, ref, down_send.at[0, i], down_recv.at[0, i], f, far)
 
     def down_on(i):
-        ref = dout.at[pl.ds(i * cut, cut), fblock]
+        ref = down_cut(far, i)
         return remote(ref, ref, down_send.at[1, i], down_recv.at[1, i], f, sib)
 
     down_sib = remote(dout.at[:, block], dout.at[:, block], sibling_send, sibling_recv, f, sib)
@@ -250,14 +261,14 @@
             crossing(k, source).start()
         beside(c, k, source).start()
 
-    def accumulate(j, source):
+    def accumulate(j, source, gs=(0, 1)):
         at, size = spans[j]
-        for k in groups[j]:
-            beside(1 - c, k, source).wait_recv()
         left = nrm[j, source, :, pl.ds(0, size)]
-
-        @pl.loop(0, 2)
-        def _(g):
+        for g in gs:
+            @pl.when(c != g)
+            def _():
+                for k in groups[j]:
+                    beside(g, k, source).wait_recv()
             acc[g] += jnp.dot(left, out[g, pl.ds(pl.multiple_of(source * rows + at, 16), size), :],
                               preferred_element_type=jnp.float32)
 
@@ -304,7 +315,8 @@
             def _(i):
                 accumulate(1, i)
     pass_on(at_home, range(DOWN_CUTS))
-    pass_on(jnp.logical_not(at_home), range(DOWN_CUTS // 2))
+    away = jnp.logical_not(at_home)
+    pass_on(away, (0, 1))
     for k in one_way:
         @pl.when(jnp.logical_not(side(k)))
         def _():
@@ -319,77 +331,99 @@
 
     @pl.loop(0, half)
     def _(i):
-        arrive(late[-1], turned + i, False)
         accumulate(2, same + i)
-
-    @pl.loop(0, half)
-    def _(i):
-        accumulate(2, turned + i)
+    for g in range(2):
+        @pl.when(c == g)
+        def _():
+            @pl.loop(0, half)
+            def _(i):
+                arrive(late[-1], turned + i, False)
+
+        @pl.loop(0, half)
+        def _(i):
+            accumulate(2, turned + i, (g,))
 
     hidden[...] = (jax.nn.silu(acc[0]) * acc[1]).astype(hidden.dtype)
     down_sib.wait_recv()
 
-    def sums(to):
-        at = pl.multiple_of(to * block_width, block_width)
-        return jnp.dot(hidden[...], dout[:, pl.ds(at, block_width)], preferred_element_type=jnp.float32)
+    share = block_width // HALVES
+    halves = [pl.ds(h * share, share) for h in range(HALVES)]
+
+    def sums(to, h):
+        at = pl.multiple_of(to * block_width + h * share, share)
+        return jnp.dot(hidden[...], dout[:, pl.ds(at, share)], preferred_element_type=jnp.float32)
 
     order = (3, 2, 1, 0)
     level = {3: 3 - z, 2: lax.rem(z + 2, 4), 1: z + 1 - 2 * lax.rem(z, 2), 0: z}
-    def collect(cond):
+
+    def collect(cond, cuts):
         @pl.when(cond)
         def _():
-            for i in range(DOWN_CUTS):
+            for i in cuts:
                 down_on(i).wait_recv()
 
-    share = tokens // HALVES
-    halves = [pl.ds(h * share, share) for h in range(HALVES)]
-
     def across(m, h):
-        return remote(pcross.at[m, halves[h]], ybuf.at[m, halves[h]], ysend.at[m, h], yrecv.at[m, h], 2 * z + 1 - y, t)
+        return remote(pcross.at[m, :, halves[h]], ybuf.at[m, :, halves[h]], ysend.at[m, h], yrecv.at[m, h],
+                      2 * z + 1 - y, t)
 
     def along(m, h):
-        return remote(sbuf.at[m, halves[h]], zbuf.at[m, halves[h]], zsend.at[m, h], zrecv.at[m, h], 2 * level[m] + y, t)
-
-    def theirs(m):
-        pcross[m] = sums(2 * level[m] + 1 - y).astype(pcross.dtype)
-
-    def ours(m):
-        pown[m] = sums(2 * level[m] + y)
-
-    def offer(m):
-        for h in range(HALVES):
-            across(m, h).start()
-
-    def pair(m):
-        for h, some in enumerate(halves):
-            across(m, h).wait_recv()
-            total = pown[m, some] + ybuf[m, some].astype(jnp.float32)
-            if m:
-                sbuf[m, some] = total.astype(sbuf.dtype)
-                along(m, h).start()
-            else:
-                pown[m, some] = total
-
-    collect(at_home)
-    theirs(3)
-    theirs(2)
-    offer(3)
-    ours(3)
-    offer(2)
-    ours(2)
-    pair(3)
-    pass_on(jnp.logical_not(at_home), range(DOWN_CUTS // 2, DOWN_CUTS))
-    collect(jnp.logical_not(at_home))
-    theirs(1)
-    theirs(0)
-    offer(1)
-    ours(1)
-    offer(0)
-    ours(0)
-    for m in (2, 1, 0):
-        pair(m)
+        return remote(sbuf.at[m, :, halves[h]], zbuf.at[m, :, halves[h]], zsend.at[m, h], zrecv.at[m, h],
+                      2 * level[m] + y, t)
+
+    def theirs(m, h):
+        pcross[m, :, halves[h]] = sums(2 * level[m] + 1 - y, h).astype(pcross.dtype)
+
+    def ours(m, h):
+        pown[m, :, halves[h]] = sums(2 * level[m] + y, h)
+
+    def pair(m, h):
+        some = halves[h]
+        across(m, h).wait_recv()
+        total = pown[m, :, some] + ybuf[m, :, some].astype(jnp.float32)
+        if m:
+            sbuf[m, :, some] = total.astype(sbuf.dtype)
+            along(m, h).start()
+        else:
+            pown[m, :, some] = total
+
+    collect(at_home, range(DOWN_CUTS))
+    first = [(3, 0), (3, 1), (2, 0), (2, 1), (1, 0), (0, 0)]
+    second = [(1, 1), (0, 1)]
+    for i, step in enumerate(first[:4]):
+        theirs(*step)
+        if i:
+            across(*first[i - 1]).start()
+    ours(*first[0])
+    across(*first[3]).start()
+    pass_on(away, range(2, DOWN_CUTS // 2))
+    for step in first[1:4]:
+        ours(*step)
+    collect(away, range(DOWN_CUTS // 2))
+    pair(*first[0])
+    pass_on(away, (DOWN_CUTS // 2,))
+    theirs(*first[4])
+    theirs(*first[5])
+    across(*first[4]).start()
+    ours(*first[4])
+    across(*first[5]).start()
+    ours(*first[5])
+    pair(*first[1])
+    pass_on(away, (DOWN_CUTS // 2 + 1,))
+    pair(*first[2])
+    pass_on(away, (DOWN_CUTS // 2 + 2,))
+    pair(*first[3])
+    pass_on(away, range(DOWN_CUTS // 2 + 3, DOWN_CUTS))
+    collect(away, range(DOWN_CUTS // 2, DOWN_CUTS))
+    for step in second:
+        theirs(*step)
+    across(*second[0]).start()
+    ours(*second[0])
+    across(*second[1]).start()
+    ours(*second[1])
+    for step in first[4:] + second:
+        pair(*step)
     total = pown[0]
-    for m in (1, 3, 2):
+    for m in (3, 2, 1):
         for h in range(HALVES):
             along(m, h).wait_recv()
         total += zbuf[m].astype(jnp.float32)

time: 253 us -> 250 us (0.988)
  Pallas kernels: 252 us -> 249 us
    pallas_call x1, Pallas kernels: 240 us -> 237 us  [layer(): pl.pallas_call(functools.partial(layer_kernel, fs, tp, plan, pieces), out...]
where the time goes in v3:
time: 250 us
  Pallas kernels  249 us (100%)
    pallas_call x1, Pallas kernels, layer(): pl.pallas_call(functools.partial(layer_kernel, fs, tp, plan, pieces), out...  237 us
    pallas_call x2, Pallas kernels, deliver(): pl.pallas_call(functools.partial(deliver_kernel, pairs), out_shape=tuple(...  12.2 us

profile of v3, /device:TPU:0, one launch (start us, length us, event | category | flops | bytes accessed | tf_op | source)
XLA Modules:
  0.0 249.6 jit_solution(5363332721509140376)
XLA Ops:
  0.6 236.8 %shard_map.84 = (bf16[2,4096,1408]{2,1,0:T(8,128)(2,1)S(1)}, bf16[1408,4096]{1,0:T(8,128)(2,1)S(1)}, bf16[192,512]{1,0:T(8,128)(2,1)S(1)}, bf16[2,512,2816]{2,1,0:T(8,128)(2,1)}) custom-call(bf16[192,4096]{1,0:T(8,128)(2,1)} %tok_hbm.1, f32[1,512]{1,0:T(1,128)} %bitcast.1, f32[512,2816]{1,0:T(8,128)} %gate_f32.1, f32[512,2816]{1,0:T(8,128)} %up_f32.1, ...), custom_call_target="tpu_custom_call" | custom-call | tf_op jit(solution)/shard_map/pallas_call | solution.py:470
  237.4 7.9 %shard_map.85 = (bf16[4096,1408]{1,0:T(8,128)(2,1)}, bf16[4096,1408]{1,0:T(8,128)(2,1)}) custom-call(bf16[2,4096,1408]{2,1,0:T(8,128)(2,1)S(1)} %get-tuple-element.11.refs_0_), custom_call_target="tpu_custom_call" | custom-call | tf_op jit(solution)/shard_map/pallas_call | solution.py:519
  245.3 4.3 %shard_map.86 = (bf16[1408,4096]{1,0:T(8,128)(2,1)}, bf16[192,512]{1,0:T(8,128)(2,1)}) custom-call(bf16[1408,4096]{1,0:T(8,128)(2,1)S(1)} %get-tuple-element.14.refs_0_, bf16[192,512]{1,0:T(8,128)(2,1)S(1)} %get-tuple-element.15.refs_1_), custom_call_target="tpu_custom_call" | custom-call | tf_op jit(solution)/shard_map/pallas_call | solution.py:519

commit v4 on v3

--- a/solution.py
+++ b/solution.py
@@ -9,37 +9,46 @@
 
 MESH = pl.DeviceIdType.MESH
 HOME, AWAY, BOTH = 0, 1, 2
-LAYER_VMEM = 27 * 2 ** 20
+LAYER_VMEM = 29 * 2 ** 20
 EARLY_RELAY = 8
 EARLY_CASTS = 2
 
 
-SHARES = ((1, AWAY), (2, BOTH), (4, AWAY), (7, HOME), (2, AWAY), (6, BOTH), (6, BOTH), (4, BOTH))
+WAYS = (AWAY, BOTH, AWAY, HOME, AWAY, BOTH, BOTH, BOTH)
+SHARES = ((1, 2, 4, 7, 2, 6, 6, 4), (1, 2, 4, 8, 2, 5, 6, 4))
 DOWN_CUTS = 8
 HALVES = 2
 
 
-def chunk_plan(rows):
-    unit = max(16, rows // sum(share for share, _ in SHARES) // 16 * 16)
-    sizes = [share * unit for share, _ in SHARES]
+def chunk_plan(rows, shares):
+    unit = max(16, rows // sum(shares) // 16 * 16)
+    sizes = [share * unit for share in shares]
     sizes[-1] += rows - sum(sizes)
-    at, plan = 0, [None] * len(SHARES)
+    at, plan = 0, [None] * len(shares)
     for both in (False, True):
-        for i, (_, way) in enumerate(SHARES):
+        for i, way in enumerate(WAYS):
             if (way == BOTH) == both:
-                plan[i] = (at, sizes[i], way)
+                plan[i] = (at, sizes[i])
                 at += sizes[i]
     return tuple(plan)
 
 
-def groups_of(plan):
-    one_way = [k for k, (_, _, way) in enumerate(plan) if way != BOTH]
-    both_ways = [k for k, (_, _, way) in enumerate(plan) if way == BOTH]
+def groups():
+    one_way = [k for k, way in enumerate(WAYS) if way != BOTH]
+    both_ways = [k for k, way in enumerate(WAYS) if way == BOTH]
     middle = len(both_ways) // 2
     return one_way, both_ways[:middle], both_ways[middle:]
 
 
-def layer_kernel(fs, tp, plan, pieces, tok_hbm, gain, gate_f32, up_f32, down_f32,
+def spans_of(plans):
+    def span(plan, group):
+        return plan[group[0]][0], sum(plan[k][1] for k in group)
+
+    spans = [[span(plan, group) for plan in plans] for group in groups()]
+    return spans, sorted({pair for both in spans for pair in both})
+
+
+def layer_kernel(fs, tp, plans, pieces, tok_hbm, gain, gate_f32, up_f32, down_f32,
                  out, dout, mixed, part, w, gcol, stage, dstage, tok, scale, nrm, acc, hidden,
                  pcross, pown, ybuf, sbuf, zbuf,
                  part_send, part_recv, own_send, relay_send, land_recv,
@@ -58,15 +67,15 @@
     planes = fs // 2
     half = fs // 2
     sib, far = 2 * x + 1 - c, 2 * (1 - x) + c
-    chunks = len(plan)
+    chunks = len(WAYS)
     slots = stage.shape[0]
-    groups = groups_of(plan)
-    spans = [(plan[group[0]][0], sum(plan[k][1] for k in group)) for group in groups]
+    one_way, early, late = groups()
+    spans, lefts = spans_of(plans)
     casts = [(k, g) for k in range(chunks) for g in range(2)]
 
     def fetch(i):
         k, g = casts[i]
-        at, size, _ = plan[k]
+        at, size = plans[g][k]
         return pltpu.make_async_copy(
             source_f32[g].at[pl.ds(at, size), :], stage.at[i % slots, pl.ds(0, size), :], stage_sem.at[i % slots])
 
@@ -112,7 +121,7 @@
         sent.append((cond, copy))
 
     def to_serve(view, sems, k, cond, home, g):
-        at, size, _ = plan[k]
+        at, size = plans[g][k]
         for yy in range(2):
             to = 2 * home + yy
             here = jnp.logical_and(to == f, c == g)
@@ -122,13 +131,13 @@
                 sems.at[g, yy, k], land_recv.at[f, k], to, 2 * x + g))
 
     def part_copy(g, k):
-        at, size, _ = plan[k]
+        at, size = plans[g][k]
         return remote(w.at[g, pl.ds(at, size), :], part.at[g, pl.ds(at, size), :],
                       part_send.at[g, k], part_recv.at[g, k], f, far)
 
     def cast(i):
         k, g = casts[i]
-        at, size, _ = plan[k]
+        at, size = plans[g][k]
         fetch(i).wait()
 
         @pl.loop(0, size // 16)
@@ -143,12 +152,12 @@
 
     def give(i):
         k, g = casts[i]
-        send(uses(own_cross, plan[k][2], HOME), part_copy(g, k))
-        if plan[k][2] != AWAY:
+        send(uses(own_cross, WAYS[k], HOME), part_copy(g, k))
+        if WAYS[k] != AWAY:
             to_serve(lambda r, q: w.at[g, r, q], own_send, k, own_cross, t, g)
 
     def relay(k):
-        come = uses(part_cross, plan[k][2], HOME)
+        come = uses(part_cross, WAYS[k], HOME)
 
         @pl.when(come)
         def _():
@@ -196,7 +205,8 @@
     cut = features // fs * 2 // DOWN_CUTS
 
     def down_cut(home, i):
-        at = home * dcols + i % 2 * block_width + i // 2 * cut
+        kind, at = divmod(i, DOWN_CUTS // 2)
+        at = home * dcols + (y if kind else 1 - y) * block_width + at * cut
         return dout.at[:, pl.ds(pl.multiple_of(at, 128), cut)]
 
     def down_far(i):
@@ -216,7 +226,7 @@
     def _(s):
         v = tok[:, pl.ds(pl.multiple_of(s * rows, rows), rows)].astype(jnp.float32)
         v = (v * scale[...]).astype(nrm.dtype)
-        for j, (at, size) in enumerate(spans):
+        for j, (at, size) in enumerate(lefts):
             nrm[j, s, :, pl.ds(0, size)] = v[:, at:at + size]
     acc[...] = jnp.zeros_like(acc)
 
@@ -242,11 +252,11 @@
             out[c, pl.ds(to, 16), :] = w[c, pl.ds(r, 16), pl.ds(pl.multiple_of(y * width, 128), width)]
 
     def landed(g, k, source):
-        at, size, _ = plan[k]
+        at, size = plans[g][k]
         return out.at[g, pl.ds(pl.multiple_of(source * rows + at, 16), size), :]
 
-    def crossing(k, source):
-        ref = landed(c, k, source)
+    def crossing(g, k, source):
+        ref = landed(g, k, source)
         return remote(ref, ref, cross_send.at[source, k], land_recv.at[source, k], f, far)
 
     def beside(g, k, source):
@@ -254,21 +264,25 @@
         return remote(ref, ref, sib_send.at[source, k], sib_recv.at[source, k], f, sib)
 
     def arrive(k, source, cross):
-        @pl.when(jnp.logical_not(jnp.logical_and(keeps, f == source)))
-        def _():
-            crossing(k, source).wait_recv()
-        if cross:
-            crossing(k, source).start()
-        beside(c, k, source).start()
+        for g in range(2):
+            @pl.when(jnp.logical_and(c == g, jnp.logical_not(jnp.logical_and(keeps, f == source))))
+            def _():
+                crossing(g, k, source).wait_recv()
+
+            @pl.when(c == g)
+            def _():
+                if cross:
+                    crossing(g, k, source).start()
+                beside(g, k, source).start()
 
     def accumulate(j, source, gs=(0, 1)):
-        at, size = spans[j]
-        left = nrm[j, source, :, pl.ds(0, size)]
         for g in gs:
             @pl.when(c != g)
             def _():
-                for k in groups[j]:
+                for k in groups()[j]:
                     beside(g, k, source).wait_recv()
+            at, size = spans[j][g]
+            left = nrm[lefts.index((at, size)), source, :, pl.ds(0, size)]
             acc[g] += jnp.dot(left, out[g, pl.ds(pl.multiple_of(source * rows + at, 16), size), :],
                               preferred_element_type=jnp.float32)
 
@@ -276,7 +290,7 @@
     turned = half - same
 
     def side(k):
-        return at_home if plan[k][2] == HOME else jnp.logical_not(at_home)
+        return at_home if WAYS[k] == HOME else jnp.logical_not(at_home)
 
     def pass_on(cond, cuts):
         for i in cuts:
@@ -285,7 +299,6 @@
                 down_far(i).wait_recv()
             send(cond, down_on(i))
 
-    one_way, early, late = groups
     for k in one_way:
         @pl.when(side(k))
         def _():
@@ -386,42 +399,43 @@
         else:
             pown[m, :, some] = total
 
+    quarter = DOWN_CUTS // 4
     collect(at_home, range(DOWN_CUTS))
-    first = [(3, 0), (3, 1), (2, 0), (2, 1), (1, 0), (0, 0)]
-    second = [(1, 1), (0, 1)]
-    for i, step in enumerate(first[:4]):
+    first = [(3, 0), (3, 1), (2, 0), (2, 1)]
+    second = [(1, 0), (1, 1), (0, 0), (0, 1)]
+    for i, step in enumerate(first):
         theirs(*step)
         if i:
             across(*first[i - 1]).start()
     ours(*first[0])
     across(*first[3]).start()
-    pass_on(away, range(2, DOWN_CUTS // 2))
-    for step in first[1:4]:
-        ours(*step)
-    collect(away, range(DOWN_CUTS // 2))
-    pair(*first[0])
-    pass_on(away, (DOWN_CUTS // 2,))
-    theirs(*first[4])
-    theirs(*first[5])
-    across(*first[4]).start()
-    ours(*first[4])
-    across(*first[5]).start()
-    ours(*first[5])
-    pair(*first[1])
-    pass_on(away, (DOWN_CUTS // 2 + 1,))
-    pair(*first[2])
-    pass_on(away, (DOWN_CUTS // 2 + 2,))
-    pair(*first[3])
-    pass_on(away, range(DOWN_CUTS // 2 + 3, DOWN_CUTS))
-    collect(away, range(DOWN_CUTS // 2, DOWN_CUTS))
-    for step in second:
+    pass_on(away, range(quarter, 2 * quarter))
+    ours(*first[1])
+    collect(away, range(2 * quarter))
+    for i, step in enumerate(second):
         theirs(*step)
-    across(*second[0]).start()
-    ours(*second[0])
-    across(*second[1]).start()
-    ours(*second[1])
-    for step in first[4:] + second:
-        pair(*step)
+        if i:
+            across(*second[i - 1]).start()
+    ours(*first[2])
+    across(*second[3]).start()
+    ours(*first[3])
+    pair(3, 0)
+    pair(3, 1)
+    pass_on(away, range(2 * quarter, 3 * quarter))
+    pair(2, 0)
+    collect(away, range(2 * quarter, 3 * quarter))
+    ours(1, 0)
+    ours(0, 0)
+    pair(2, 1)
+    pass_on(away, range(3 * quarter, 4 * quarter - 1))
+    pair(1, 0)
+    pass_on(away, range(4 * quarter - 1, 4 * quarter))
+    collect(away, range(3 * quarter, 4 * quarter))
+    ours(1, 1)
+    pair(1, 1)
+    ours(0, 1)
+    pair(0, 0)
+    pair(0, 1)
     total = pown[0]
     for m in (3, 2, 1):
         for h in range(HALVES):
@@ -438,16 +452,19 @@
         @pl.when(cond)
         def _():
             copy.wait_send()
-    for k in range(chunks):
-        @pl.loop(0, fs)
-        def _(i):
-            beside(c, k, i).wait_send()
-        if plan[k][2] != BOTH:
-            @pl.when(side(k))
-            def _():
-                @pl.loop(0, half)
+    for g in range(2):
+        @pl.when(c == g)
+        def _():
+            for k in range(chunks):
+                @pl.loop(0, fs)
                 def _(i):
-                    crossing(k, turned + i).wait_send()
+                    beside(g, k, i).wait_send()
+                if WAYS[k] != BOTH:
+                    @pl.when(side(k))
+                    def _():
+                        @pl.loop(0, half)
+                        def _(i):
+                            crossing(g, k, turned + i).wait_send()
 
 
 def layer(tok, gain, gate, up, down, fs, tp):
@@ -457,18 +474,19 @@
     features = dcols * tp
     tokens = tok.shape[0]
     block_width = features // fs
-    plan = chunk_plan(rows)
-    n = len(plan)
-    widest = max(size for _, size, _ in plan)
+    plans = tuple(chunk_plan(rows, shares) for shares in SHARES)
+    n = len(WAYS)
+    widest = max(size for plan in plans for _, size in plan)
+    lefts = spans_of(plans)[1]
     pieces = 8
-    deepest = max(-(-sum(plan[k][1] for k in group) // 128) * 128 for group in groups_of(plan))
+    deepest = max(-(-size // 128) * 128 for _, size in lefts)
     bf16 = jnp.bfloat16
     dma = pltpu.SemaphoreType.DMA
     hbm = pl.BlockSpec(memory_space=pltpu.HBM)
     vmem = pl.BlockSpec(memory_space=pltpu.VMEM)
     slots = pltpu.VMEM((fs // 2, tokens, block_width), bf16)
     return pl.pallas_call(
-        functools.partial(layer_kernel, fs, tp, plan, pieces),
+        functools.partial(layer_kernel, fs, tp, plans, pieces),
         out_shape=(
             pltpu.VMEM((2, rows * fs, width), bf16),
             pltpu.VMEM((units, features), bf16),
@@ -484,7 +502,7 @@
             pltpu.VMEM((2, units // pieces, dcols), jnp.float32),
             pltpu.VMEM(tok.shape, bf16),
             pltpu.VMEM((tokens, 1), jnp.float32),
-            pltpu.VMEM((3, fs, tokens, deepest), bf16),
+            pltpu.VMEM((len(lefts), fs, tokens, deepest), bf16),
             pltpu.VMEM((2, tokens, width), jnp.float32),
             pltpu.VMEM((tokens, width), bf16),
             slots, pltpu.VMEM((fs // 2, tokens, block_width), jnp.float32), slots, slots, slots,

time: 250 us -> 247 us (0.988)
  Pallas kernels: 249 us -> 246 us
    pallas_call x1, Pallas kernels: 237 us -> 234 us  [layer(): pl.pallas_call(functools.partial(layer_kernel, fs, tp, plans, pieces), ou...]
where the time goes in v4:
time: 247 us
  Pallas kernels  246 us (100%)
    pallas_call x1, Pallas kernels, layer(): pl.pallas_call(functools.partial(layer_kernel, fs, tp, plans, pieces), ou...  234 us
    pallas_call x2, Pallas kernels, deliver(): pl.pallas_call(functools.partial(deliver_kernel, pairs), out_shape=tuple(...  12.2 us

profile of v4, /device:TPU:0, one launch (start us, length us, event | category | flops | bytes accessed | tf_op | source)
XLA Modules:
  0.0 247.0 jit_solution(10412727591000391130)
XLA Ops:
  0.6 234.1 %shard_map.84 = (bf16[2,4096,1408]{2,1,0:T(8,128)(2,1)S(1)}, bf16[1408,4096]{1,0:T(8,128)(2,1)S(1)}, bf16[192,512]{1,0:T(8,128)(2,1)S(1)}, bf16[2,512,2816]{2,1,0:T(8,128)(2,1)}) custom-call(bf16[192,4096]{1,0:T(8,128)(2,1)} %tok_hbm.1, f32[1,512]{1,0:T(1,128)} %bitcast.1, f32[512,2816]{1,0:T(8,128)} %gate_f32.1, f32[512,2816]{1,0:T(8,128)} %up_f32.1, ...), custom_call_target="tpu_custom_call" | custom-call | tf_op jit(solution)/shard_map/pallas_call | solution.py:488
  234.8 7.9 %shard_map.85 = (bf16[4096,1408]{1,0:T(8,128)(2,1)}, bf16[4096,1408]{1,0:T(8,128)(2,1)}) custom-call(bf16[2,4096,1408]{2,1,0:T(8,128)(2,1)S(1)} %get-tuple-element.11.refs_0_), custom_call_target="tpu_custom_call" | custom-call | tf_op jit(solution)/shard_map/pallas_call | solution.py:537
  242.7 4.3 %shard_map.86 = (bf16[1408,4096]{1,0:T(8,128)(2,1)}, bf16[192,512]{1,0:T(8,128)(2,1)}) custom-call(bf16[1408,4096]{1,0:T(8,128)(2,1)S(1)} %get-tuple-element.14.refs_0_, bf16[192,512]{1,0:T(8,128)(2,1)S(1)} %get-tuple-element.15.refs_1_), custom_call_target="tpu_custom_call" | custom-call | tf_op jit(solution)/shard_map/pallas_call | solution.py:537
